TPU v7x, 32 devices: a whole 2x2x4 slice. The times are simulated.
32 devices in a mesh: sp: 16 (over z, y, x), tp: 2 (over core).
Axes of the slice: x: 2, y: 2, z: 4, core: 2. Of those that a mesh axis runs over, the one named last changes fastest.
Arguments:
- prompt: bfloat16 [16, 1024, 2048], P('sp', None, 'tp'), may hold values from -6 to 6
- new_input: bfloat16 [16, 2048], P('sp', 'tp'), may hold values from -140 to 140
- w_query: bfloat16 [2048, 2048], P('sp', 'tp'), may hold values from -0.21875 to 0.21875
- w_key: bfloat16 [2048, 2048], P('sp', 'tp'), may hold values from -0.125 to 0.125
- w_value: bfloat16 [2048, 2048], P('sp', 'tp'), may hold values from -0.125 to 0.125
- lam: float32 [16], P('tp'), may hold values from 0.3 to 0.8
- out_gain: float32 [128], replicated, may hold values from 0.1 to 1.9
Outputs:
- key_cache: bfloat16 [16, 1024, 2048], P('sp', None, 'tp')
- value_cache: bfloat16 [16, 1024, 2048], P('sp', None, 'tp')
- first_read: bfloat16 [16, 16, 128], P('sp', 'tp')
All inputs are finite; a program needn't handle non-finite values.
Results may differ from a plain program's by a relative error of at most 0.02.
The roundings to bfloat16 on the way count: a program that leaves them out, or rounds other values in their place, can miss the bound.
Values may be sent and summed in bfloat16 or wider, within the bound.
A program may use at most 64 MiB of HBM per device.

v0:
```python
import jax
import jax.numpy as jnp
from jax import lax
from jax.sharding import PartitionSpec as P

MAP_DIM = 64
VAL_DIM = 128
LEN = 1024
rope_base = 500000.0
norm_eps = 1e-05


def rotate(vectors, angle):
    half = vectors.shape[-1] // 2
    cosine_table = jnp.cos(angle)
    sine = jnp.sin(angle)
    first = vectors[..., :half]
    second = vectors[..., half:]
    return jnp.concatenate(
        [first * cosine_table - second * sine, second * cosine_table + first * sine], axis=-1
    )


def inverse_freq():
    return rope_base ** (-(jnp.arange(MAP_DIM // 2, dtype=jnp.float32) * 2.0 / MAP_DIM))


def finish(mixed, lam, out_gain):
    diff = mixed[:, :, 0] - lam[None, :, None] * mixed[:, :, 1]
    normed = diff * lax.rsqrt(jnp.mean(diff * diff, axis=-1, keepdims=True) + norm_eps)
    return (normed * out_gain).astype(jnp.bfloat16)


def read_whole(query, keys, values, lam, out_gain):
    seqs, length, _ = keys.shape
    heads = lam.shape[0]
    key_maps = keys.reshape(seqs, length, heads, 2, MAP_DIM)
    value_heads = values.reshape(seqs, length, heads, VAL_DIM)
    attention_scores = jnp.einsum(
        "shmd,slhmd->shml", query, key_maps, preferred_element_type=jnp.float32
    ) * MAP_DIM ** (-0.5)
    weights = jax.nn.softmax(attention_scores, axis=-1)
    mixed = jnp.einsum(
        "shml,slhe->shme", weights, value_heads.astype(jnp.float32), precision=lax.Precision.HIGHEST
    )
    return finish(mixed, lam, out_gain)


def body(prompt, new_input, w_query, w_key, w_value, lam, out_gain):
    heads = lam.shape[0]
    seqs, count, _ = prompt.shape
    local_seqs = new_input.shape[0]
    inverse = inverse_freq()
    full_query, full_key, full_value = (
        lax.all_gather(w_query, "sp", axis=0, tiled=True),
        lax.all_gather(w_key, "sp", axis=0, tiled=True),
        lax.all_gather(w_value, "sp", axis=0, tiled=True),
    )
    pieces = (
        lax.all_gather(prompt, "tp", axis=2, tiled=True),
        lax.all_gather(new_input[:, None, :], "tp", axis=2, tiled=True),
    )
    width_piece = pieces[0].shape[2]
    row_piece = pieces[0].reshape(seqs * count, width_piece)
    fresh_piece = pieces[1][:, 0, :]
    key_sum = jnp.dot(row_piece, full_key, preferred_element_type=jnp.float32)
    weighted_value_sum = jnp.dot(row_piece, full_value, preferred_element_type=jnp.float32)
    query_sum = jnp.dot(fresh_piece, full_query, preferred_element_type=jnp.float32)
    positions = jnp.arange(count, dtype=jnp.float32)
    key_maps = rotate(
        key_sum.reshape(seqs, count, heads, 2, MAP_DIM), positions[:, None, None, None] * inverse
    )
    keys = key_maps.astype(jnp.bfloat16).reshape(seqs, count, heads * 2 * MAP_DIM)
    values = weighted_value_sum.astype(jnp.bfloat16).reshape(seqs, count, heads * VAL_DIM)
    query = rotate(
        query_sum.reshape(local_seqs, heads, 2, MAP_DIM), jnp.float32(LEN) * inverse
    ).astype(jnp.bfloat16)
    first_read = read_whole(query, keys, values, lam, out_gain)
    return (keys, values, first_read)


def solution(mesh):
    in_specs = (
        P("sp", None, "tp"),
        P("sp", "tp"),
        P("sp", "tp"),
        P("sp", "tp"),
        P("sp", "tp"),
        P("tp"),
        P(),
    )
    out_specs = (P("sp", None, "tp"), P("sp", None, "tp"), P("sp", "tp", None))
    return jax.shard_map(body, mesh=mesh, in_specs=in_specs, out_specs=out_specs, check_vma=False)
```

profile of v0, /device:TPU:0, one launch (start us, length us, event | category | flops | bytes accessed | tf_op | source)
XLA Modules:
  0.0 297.6 jit_solution(11442602501516390730)
XLA Ops:
  7.2 0.0 all-gather.8.cloned.1.call-start
  7.2 0.7 all-gather.8.cloned.1.call-update
  7.9 0.0 all-gather.12.cloned.1.call-start
  7.9 1.8 copy.16
  9.8 0.0 all-gather.6.cloned.1.call-start
  9.8 0.7 all-gather.6.cloned.1.call-update
  10.5 0.0 all-gather.10.cloned.1.call-start
  10.5 0.5 all-gather.10.cloned.1.call-update
  11.1 2.1 all-gather
  13.2 0.1 multiply_sine_fusion
  13.2 0.5 fusion.15
  13.8 75.3 %all-gather.8.cloned.1.call-done = bf16[2048,1024]{1,0:T(8,128)(2,1)} async-done(((bf16[128,1024]{1,0:T(8,128)(2,1)}), bf16[2048,1024]{1,0:T(8,128)(2,1)}) %all-gather.8.cloned.1.call-update) | async-done | bytes 4194320 | tf_op jit(solution)/shard_map/all_gather | solution.py:56
  89.1 6.5 %copy.15 = bf16[1024,2048]{1,0:T(8,128)(2,1)} copy(bf16[1024,2048]{0,1:T(8,128)(2,1)} %bitcast.59) | data formatting | bytes 8388608 | tf_op jit(solution)/shard_map/dot_general | solution.py:66
  95.6 84.1 %all-gather.12.cloned.1.call-done = bf16[2048,1024]{0,1:T(8,128)(2,1)} async-done(((bf16[128,1024]{0,1:T(8,128)(2,1)}), bf16[2048,1024]{0,1:T(8,128)(2,1)}) %all-gather.12.cloned.1.call-update) | async-done | bytes 4194320 | tf_op jit(solution)/shard_map/all_gather | solution.py:55
  179.7 3.9 %fusion.20 = f32[1,8,2,64]{3,0,2,1:T(1,128)S(1)} fusion(bf16[8,2,64,2048]{3,2,1,0:T(8,128)(2,1)} %bitcast.60, bf16[1,2048]{1,0:T(2,128)(2,1)S(1)} %all-gather), kind=kOutput, calls=%fused_computation.23 | convolution fusion | flops 4194304 | bytes 4202496 | tf_op jit(solution)/shard_map/dot_general | solution.py:68
  183.6 0.1 fusion.23
  183.7 0.1 maximum_bitcast_fusion
  183.8 9.3 %all-gather.6.cloned.1.call-done = bf16[1,1024,2048]{2,1,0:T(8,128)(2,1)} async-done(((bf16[1,1024,1024]{2,1,0:T(8,128)(2,1)}), bf16[1,1024,2048]{2,1,0:T(8,128)(2,1)}) %all-gather.6.cloned.1.call-update) | async-done | bytes 4194320 | tf_op jit(solution)/shard_map/all_gather | solution.py:60
  193.1 7.6 %fusion.4 = f32[1,1024,8,2,64]{1,4,3,2,0:T(8,128)S(1)} fusion(bf16[8,2,64,2048]{3,2,1,0:T(8,128)(2,1)} %bitcast.61, bf16[1,1024,2048]{2,1,0:T(8,128)(2,1)} %all-gather.6.cloned.1.call-done), kind=kOutput, calls=%fused_computation.4 | convolution fusion | flops 4294967296 | bytes 12582912 | tf_op jit(solution)/shard_map/dot_general | solution.py:66
  200.7 0.7 subtract_convert_fusion
  201.5 0.4 fusion.7
  201.9 0.1 fusion.25
  202.0 0.2 fusion.17
  202.2 0.2 pad_maximum_fusion
  202.4 70.2 %all-gather.10.cloned.1.call-done = bf16[2048,1024]{1,0:T(8,128)(2,1)} async-done(((bf16[128,1024]{1,0:T(8,128)(2,1)}), bf16[2048,1024]{1,0:T(8,128)(2,1)}) %all-gather.10.cloned.1.call-update) | async-done | bytes 4194320 | tf_op jit(solution)/shard_map/all_gather | solution.py:57
  272.6 8.0 %fusion.11 = bf16[1024,1024]{0,1:T(8,128)(2,1)S(1)} fusion(bf16[2048,1024]{1,0:T(8,128)(2,1)} %all-gather.10.cloned.1.call-done, bf16[1,1024,2048]{2,1,0:T(8,128)(2,1)} %all-gather.6.cloned.1.call-done), kind=kOutput, calls=%fused_computation.12 | convolution fusion | flops 4296015872 | bytes 10485760 | tf_op jit(solution)/shard_map/dot_general | solution.py:67
  280.6 1.3 copy-done
  281.9 1.8 convolution_bitcast_fusion
  283.7 0.2 multiply_reduce_fusion
  283.9 2.6 copy.19
  286.5 3.9 %copy.20 = bf16[1,1024,1024]{2,1,0:T(8,128)(2,1)} copy(bf16[1,1024,1024]{1,2,0:T(8,128)(2,1)} %bitcast.65) | data formatting | bytes 4194304
  290.4 0.7 multiply_convert_fusion
  (9 shorter events, 0.1 us)
Async XLA Ops:
  7.2 81.9 %all-gather.8.cloned.1.call-start = ((), (), s32[]{:S(2)}) async-start(), calls=%async_computation.1 | async-start | bytes 4456448 | tf_op jit(solution)/shard_map/all_gather | solution.py:56
  7.9 171.8 %all-gather.12.cloned.1.call-start = ((), (), s32[]{:S(2)}) async-start(), calls=%async_computation.3 | async-start | bytes 4456448 | tf_op jit(solution)/shard_map/all_gather | solution.py:55
  9.8 183.4 %all-gather.6.cloned.1.call-start = ((), (), s32[]{:S(2)}) async-start(), calls=%async_computation | async-start | bytes 6291456 | tf_op jit(solution)/shard_map/all_gather | solution.py:60
  10.5 262.1 %all-gather.10.cloned.1.call-start = ((), (), s32[]{:S(2)}) async-start(), calls=%async_computation.2 | async-start | bytes 4456448 | tf_op jit(solution)/shard_map/all_gather | solution.py:57
  202.4 81.3 %copy-start.1 = (f32[8]{0:T(128)S(1)}, f32[8]{0:T(128)}, u32[]{:S(2)}) copy-start(f32[8]{0:T(128)} %param.12) | copy-start | bytes 100
  280.6 1.3 copy-start
  283.9 6.5 %copy-start.2 = (f32[128]{0:T(128)S(1)}, f32[128]{0:T(128)}, u32[]{:S(2)}) copy-start(f32[128]{0:T(128)} %param.13) | copy-start | bytes 1540
Sparse Core Ops, SparseCore 0:
  10.7 78.3 all-gather.7
  92.4 87.3 all-gather.11
  181.3 11.8 all-gather.5
  195.8 76.7 all-gather.9
where the time goes:
time: 298 us
  waiting for transfers between devices  241 us (81%)
  matrix products  21.7 us (7%)
  local copies, waits for them, and re-layouts  16.1 us (5%)
  between operations  13.9 us (5%)
    all_gather x1, waiting for transfers between devices, body(): lax.all_gather(w_query, 'sp', axis=0, tiled=True)  84.1 us
    all_gather x1, waiting for transfers between devices, body(): lax.all_gather(w_key, 'sp', axis=0, tiled=True)  75.3 us
    all_gather x1, waiting for transfers between devices, body(): lax.all_gather(w_value, 'sp', axis=0, tiled=True)  70.2 us
    unnamed x9, local copies, waits for them, and re-layouts  9.62 us
    all_gather x1, waiting for transfers between devices, body(): lax.all_gather(prompt, 'tp', axis=2, tiled=True)  9.34 us
    dot_general x1, matrix products, body(): jnp.dot(row_piece, full_value, preferred_element_type=jnp.float32)  8.02 us
    dot_general x1, matrix products, body(): key_sum = jnp.dot(row_piece, full_key, preferred_element_type=jnp.float32)  7.59 us
    dot_general x1, local copies, waits for them, and re-layouts, body(): key_sum = jnp.dot(row_piece, full_key, preferred_element_type=jnp.float32)  6.5 us
  transfers between devices with their start and end apart: 4, of which 4 were waited for; matrix products, arithmetic and copies ran while one was open for 7% of the time, Pallas kernels for 0%

commit v1 on v0

--- a/solution.py
+++ b/solution.py
@@ -53,7 +53,9 @@
     inverse = inverse_freq()
     full_query, full_key, full_value = (
         lax.all_gather(w_query, "sp", axis=0, tiled=True),
-        lax.all_gather(w_key, "sp", axis=0, tiled=True),
+        jnp.concatenate(
+            lax.all_to_all(jnp.stack([w_key] * lax.axis_size("sp")), "sp", 0, 0), axis=0
+        ),
         lax.all_gather(w_value, "sp", axis=0, tiled=True),
     )
     pieces = (

time: 298 us -> 287 us (0.963)
  waiting for transfers between devices: 241 us -> 211 us
  local copies, waits for them, and re-layouts: 16.1 us -> 26.5 us
  starting transfers between devices: 0.16 us -> 8.65 us
    all_to_all x0 -> x1, waiting for transfers between devices: none -> 93.2 us  [body(): lax.all_to_all(jnp.stack([w_key] * lax.axis_size('sp')), 'sp', 0, 0)]
    all_gather x1 -> x0, waiting for transfers between devices: 75.3 us -> none  [body(): lax.all_gather(w_key, 'sp', axis=0, tiled=True)]
    all_gather x1, waiting for transfers between devices: 84.1 us -> 35.4 us  [body(): lax.all_gather(w_query, 'sp', axis=0, tiled=True)]
    all_to_all x0 -> x1, starting transfers between devices: none -> 8.52 us  [body(): lax.all_to_all(jnp.stack([w_key] * lax.axis_size('sp')), 'sp', 0, 0)]
    all_to_all x0 -> x1, local copies, waits for them, and re-layouts: none -> 6.45 us  [body(): lax.all_to_all(jnp.stack([w_key] * lax.axis_size('sp')), 'sp', 0, 0)]
    unnamed x9 -> x12, local copies, waits for them, and re-layouts: 9.62 us -> 10.7 us
  transfers between devices with their start and end apart: 4 -> 4, of which waited for: 4 -> 4; matrix products, arithmetic and copies ran while one was open for 7% -> 11% of each run, Pallas kernels for 0% -> 0%
where the time goes in v1:
time: 287 us; the launch traced here: 286 us
  waiting for transfers between devices  211 us (74%)
  local copies, waits for them, and re-layouts  26.5 us (9%)
  matrix products  21.7 us (8%)
  between operations  13.9 us (5%)
  starting transfers between devices  8.65 us (3%)
    all_to_all x1, waiting for transfers between devices, body(): lax.all_to_all(jnp.stack([w_key] * lax.axis_size('sp')), 'sp', 0, 0)  93.2 us
    all_gather x1, waiting for transfers between devices, body(): lax.all_gather(w_value, 'sp', axis=0, tiled=True)  70.3 us
    all_gather x1, waiting for transfers between devices, body(): lax.all_gather(w_query, 'sp', axis=0, tiled=True)  35.4 us
    all_gather x1, waiting for transfers between devices, body(): lax.all_gather(prompt, 'tp', axis=2, tiled=True)  10.9 us
    unnamed x12, local copies, waits for them, and re-layouts  10.7 us
    all_to_all x1, starting transfers between devices, body(): lax.all_to_all(jnp.stack([w_key] * lax.axis_size('sp')), 'sp', 0, 0)  8.52 us
    dot_general x1, matrix products, body(): jnp.dot(row_piece, full_value, preferred_element_type=jnp.float32)  8.02 us
    dot_general x1, matrix products, body(): key_sum = jnp.dot(row_piece, full_key, preferred_element_type=jnp.float32)  7.59 us
  transfers between devices with their start and end apart: 4, of which 4 were waited for; matrix products, arithmetic and copies ran while one was open for 11% of the time, Pallas kernels for 0%

profile of v1, /device:TPU:0, one launch (start us, length us, event | category | flops | bytes accessed | tf_op | source)
XLA Modules:
  0.0 286.5 jit_solution(1684135463326081648)
XLA Ops:
  7.2 1.8 copy.30
  9.1 0.7 all-gather.5.cloned.1.call-update
  9.8 1.1 copy.27
  10.9 2.8 stack.2
  13.7 8.5 %all-to-all-start = ((bf16[16,128,1024]{1,2,0:T(8,128)(2,1)}), bf16[16,128,1024]{1,2,0:T(8,128)(2,1)}, u32[]{:S(2)}, u32[]{:S(2)}) async-start(bf16[16,128,1024]{1,2,0:T(8,128)(2,1)} %stack.2), calls=%async_computation | async-start | bytes 8388608 | tf_op jit(solution)/shard_map/all_to_all | solution.py:57
  22.2 0.0 all-gather.7.cloned.1.call-start
  22.3 0.7 all-gather.7.cloned.1.call-update
  23.0 1.8 all-gather
  24.8 0.1 multiply_sine_fusion
  24.8 0.5 fusion.15
  25.4 93.2 %all-to-all-done = bf16[16,128,1024]{1,2,0:T(8,128)(2,1)} async-done(((bf16[16,128,1024]{1,2,0:T(8,128)(2,1)}), bf16[16,128,1024]{1,2,0:T(8,128)(2,1)}, u32[]{:S(2)}, u32[]{:S(2)}) %all-to-all-start) | async-done | bytes 4194336 | tf_op jit(solution)/shard_map/all_to_all | solution.py:57
  118.6 6.5 %copy.28 = bf16[16,128,1024]{2,1,0:T(8,128)(2,1)} copy(bf16[16,128,1024]{1,2,0:T(8,128)(2,1)} %all-to-all-done) | data formatting | bytes 8388608 | tf_op jit(solution)/shard_map/all_to_all | solution.py:57
  125.0 6.5 %copy.29 = bf16[1024,2048]{1,0:T(8,128)(2,1)} copy(bf16[1024,2048]{0,1:T(8,128)(2,1)} %bitcast.60) | data formatting | bytes 8388608 | tf_op jit(solution)/shard_map/dot_general | solution.py:68
  131.6 35.4 %all-gather.9.cloned.1.call-done = bf16[2048,1024]{0,1:T(8,128)(2,1)} async-done(((bf16[128,1024]{0,1:T(8,128)(2,1)}), bf16[2048,1024]{0,1:T(8,128)(2,1)}) %all-gather.9.cloned.1.call-update) | async-done | bytes 4194320 | tf_op jit(solution)/shard_map/all_gather | solution.py:55
  166.9 3.9 %fusion.20 = f32[1,8,2,64]{3,0,2,1:T(1,128)S(1)} fusion(bf16[8,2,64,2048]{3,2,1,0:T(8,128)(2,1)} %bitcast.62, bf16[1,2048]{1,0:T(2,128)(2,1)S(1)} %all-gather), kind=kOutput, calls=%fused_computation.23 | convolution fusion | flops 4194304 | bytes 4202496 | tf_op jit(solution)/shard_map/dot_general | solution.py:70
  170.8 0.1 fusion.23
  170.9 0.1 maximum_bitcast_fusion
  171.0 10.9 %all-gather.5.cloned.1.call-done = bf16[1,1024,2048]{2,1,0:T(8,128)(2,1)} async-done(((bf16[1,1024,1024]{2,1,0:T(8,128)(2,1)}), bf16[1,1024,2048]{2,1,0:T(8,128)(2,1)}) %all-gather.5.cloned.1.call-update) | async-done | bytes 4194320 | tf_op jit(solution)/shard_map/all_gather | solution.py:62
  181.9 7.6 %fusion.4 = f32[1,1024,8,2,64]{1,4,3,2,0:T(8,128)S(1)} fusion(bf16[8,2,64,2048]{3,2,1,0:T(8,128)(2,1)} %bitcast.63, bf16[1,1024,2048]{2,1,0:T(8,128)(2,1)} %all-gather.5.cloned.1.call-done), kind=kOutput, calls=%fused_computation.4 | convolution fusion | flops 4294967296 | bytes 12582912 | tf_op jit(solution)/shard_map/dot_general | solution.py:68
  189.5 0.7 subtract_convert_fusion
  190.2 0.4 fusion.7
  190.6 0.1 fusion.25
  190.7 0.2 fusion.17
  190.9 0.2 pad_maximum_fusion
  191.1 70.3 %all-gather.7.cloned.1.call-done = bf16[2048,1024]{1,0:T(8,128)(2,1)} async-done(((bf16[128,1024]{1,0:T(8,128)(2,1)}), bf16[2048,1024]{1,0:T(8,128)(2,1)}) %all-gather.7.cloned.1.call-update) | async-done | bytes 4194320 | tf_op jit(solution)/shard_map/all_gather | solution.py:59
  261.4 8.0 %fusion.11 = bf16[1024,1024]{0,1:T(8,128)(2,1)S(1)} fusion(bf16[2048,1024]{1,0:T(8,128)(2,1)} %all-gather.7.cloned.1.call-done, bf16[1,1024,2048]{2,1,0:T(8,128)(2,1)} %all-gather.5.cloned.1.call-done), kind=kOutput, calls=%fused_computation.12 | convolution fusion | flops 4296015872 | bytes 10485760 | tf_op jit(solution)/shard_map/dot_general | solution.py:69
  269.5 1.3 copy-done
  270.8 1.8 convolution_bitcast_fusion
  272.6 0.2 multiply_reduce_fusion
  272.8 2.6 copy.33
  275.4 3.9 %copy.34 = bf16[1,1024,1024]{2,1,0:T(8,128)(2,1)} copy(bf16[1,1024,1024]{1,2,0:T(8,128)(2,1)} %bitcast.67) | data formatting | bytes 4194304
  279.3 0.7 multiply_convert_fusion
  (13 shorter events, 0.1 us)
Async XLA Ops:
  7.2 159.8 %all-gather.9.cloned.1.call-start = ((), (), s32[]{:S(2)}) async-start(), calls=%async_computation.3 | async-start | bytes 4456448 | tf_op jit(solution)/shard_map/all_gather | solution.py:55
  9.0 172.8 %all-gather.5.cloned.1.call-start = ((), (), s32[]{:S(2)}) async-start(), calls=%async_computation.1 | async-start | bytes 6291456 | tf_op jit(solution)/shard_map/all_gather | solution.py:62
  13.7 9.3 %copy-start.1 = (bf16[1,1024]{1,0:T(2,128)(2,1)S(1)}, bf16[1,1024]{1,0:T(2,128)(2,1)}, u32[]{:S(2)}) copy-start(bf16[1,1024]{1,0:T(2,128)(2,1)} %param.8) | copy-start | bytes 6148
  13.7 104.9 %all-to-all-start = ((bf16[16,128,1024]{1,2,0:T(8,128)(2,1)}), bf16[16,128,1024]{1,2,0:T(8,128)(2,1)}, u32[]{:S(2)}, u32[]{:S(2)}) async-start(bf16[16,128,1024]{1,2,0:T(8,128)(2,1)} %stack.2), calls=%async_computation | async-start | bytes 8388608 | tf_op jit(solution)/shard_map/all_to_all | solution.py:57
  22.2 239.2 %all-gather.7.cloned.1.call-start = ((), (), s32[]{:S(2)}) async-start(), calls=%async_computation.2 | async-start | bytes 4456448 | tf_op jit(solution)/shard_map/all_gather | solution.py:59
  191.1 81.5 %copy-start.2 = (f32[8]{0:T(128)S(1)}, f32[8]{0:T(128)}, u32[]{:S(2)}) copy-start(f32[8]{0:T(128)} %param.12) | copy-start | bytes 100
  269.5 1.3 copy-start
  272.8 6.5 %copy-start.3 = (f32[128]{0:T(128)S(1)}, f32[128]{0:T(128)}, u32[]{:S(2)}) copy-start(f32[128]{0:T(128)} %param.13) | copy-start | bytes 1540
Sparse Core Ops, SparseCore 0:
  11.2 155.6 all-gather.8
  168.5 13.3 all-gather.4
  184.6 76.7 all-gather.6
